TPU v7x, 32 devices: a whole 2x2x4 slice. The times are simulated.
32 devices in a mesh: sp: 16 (over z, y, x), tp: 2 (over core).
Axes of the slice: x: 2, y: 2, z: 4, core: 2. Of those that a mesh axis runs over, the one named last changes fastest.
Arguments:
- queries: bfloat16 [4096, 1024], P('sp', 'tp'), may hold values from -100 to 100
- keys: bfloat16 [256, 4096], P('tp', 'sp'), may hold values from -5 to 5
- values: bfloat16 [256, 4096], P('tp', 'sp'), may hold values from -4.5 to 4.5
- gate_cache: float32 [8, 4096], P('tp', 'sp'), as said below
- documents: int32 [4096], P('sp'), may hold values from 0 to 2, never falling along the last dimension, each value on 1 to 2560 neighbouring positions
- residual: bfloat16 [4096, 2048], P(('sp', 'tp')), may hold values from -3 to 3
- out_weight: bfloat16 [1024, 2048], replicated, may hold values from -2 to 2
- mix_gain: bfloat16 [2048], replicated, may hold values from 0.099609375 to 1.8984375
- routes: int32 [4096, 4], P(('sp', 'tp')), may hold values from 0 to 31, all different within a row; in each aligned block of 128 rows (0 to 127, 128 to 255, ...) at most 32 rows name the same one
- route_weight: float32 [4096, 4], P(('sp', 'tp')), may hold values from 0.25 to 1
- expert_gate: bfloat16 [32, 2048, 512], P(('sp', 'tp')), may hold values from -0.125 to 0.125
- expert_up: bfloat16 [32, 2048, 512], P(('sp', 'tp')), may hold values from -0.125 to 0.125
- expert_down: bfloat16 [32, 512, 2048], P(('sp', 'tp')), may hold values from -0.25 to 0.25
- shared_gate: bfloat16 [2048, 512], replicated, may hold values from -0.125 to 0.125
- shared_up: bfloat16 [2048, 512], replicated, may hold values from -0.125 to 0.125
- shared_down: bfloat16 [512, 2048], replicated, may hold values from -0.25 to 0.25
- ffn_gain: bfloat16 [2048], replicated, may hold values from 0.099609375 to 1.8984375
Outputs:
- result: bfloat16 [4096, 2048], P(('sp', 'tp'))
Inputs may be any that keep to these rules, and one draw needn't show every extreme that they name: `gate_cache`: entry (h, j) is the sum of head h's log forget gates over positions 0 to j. `documents`: never falls along the positions; no document has more than 2560 positions. `routes`: each row names 4 different experts; in the rows of one device (aligned blocks of 128 rows) no expert is named more than 32 times, a bound that some block reaches.
All inputs are finite; a program needn't handle non-finite values.
Results may differ from a plain program's by a relative error of at most 0.013.
Values may be sent and summed in bfloat16 or wider, within the bound.
A program may use at most 256 MiB of HBM per device.

v0:
```python
import jax
import jax.numpy as jnp
from jax import lax
from jax.sharding import PartitionSpec as P

HD = 128
residual_scale = 2.0**0.25
norm_epsilon = 1e-05
masked_score = -1e30


def normalize(summed, gain_vector):
    row_mean = jnp.mean(summed, axis=-1, keepdims=True)
    centred = summed - row_mean
    spread = jnp.mean(centred * centred, axis=-1, keepdims=True)
    return (centred * lax.rsqrt(spread + norm_epsilon) * gain_vector.astype(jnp.float32)).astype(
        jnp.bfloat16
    )


def expert_block(arrived, expert_gate, expert_up, expert_down):
    own_count = expert_gate.shape[0]
    grouped = arrived.reshape(-1, own_count, arrived.shape[1], arrived.shape[2])
    gate_part = jnp.einsum(
        "nemd,edf->nemf", grouped, expert_gate, preferred_element_type=jnp.float32
    )
    up_part = jnp.einsum("nemd,edf->nemf", grouped, expert_up, preferred_element_type=jnp.float32)
    hidden = (jax.nn.silu(gate_part) * up_part).astype(jnp.bfloat16)
    produced = jnp.einsum("nemf,efd->nemd", hidden, expert_down, preferred_element_type=jnp.float32)
    return produced.astype(jnp.bfloat16).reshape(arrived.shape)


def local(
    queries,
    keys,
    values,
    gate_cache,
    documents,
    residual,
    out_weight,
    mix_gain,
    routes,
    route_weight,
    expert_gate,
    expert_up,
    expert_down,
    shared_gate,
    shared_up,
    shared_down,
    ffn_gain,
):
    tok_rows = queries.shape[0]
    local_heads = gate_cache.shape[0]
    kv_local = keys.shape[0] // HD
    group_size = local_heads // kv_local
    score_scale = HD ** (-0.5)
    seq_start = lax.axis_index("sp") * tok_rows
    query_pos = seq_start + jnp.arange(tok_rows, dtype=jnp.int32)
    query_last = seq_start + tok_rows - 1
    query_cum = jnp.transpose(gate_cache).reshape(tok_rows, kv_local, group_size)
    grouped_q = queries.reshape(tok_rows, kv_local, group_size, HD)
    all_cache, all_docs = (
        lax.all_gather(gate_cache, "sp", axis=1, tiled=True),
        lax.all_gather(documents.reshape(1, tok_rows), "sp", axis=1, tiled=True),
    )
    doc_line = all_docs[0]
    initial = (
        jnp.full((tok_rows, kv_local, group_size), masked_score, jnp.float32),
        jnp.zeros((tok_rows, kv_local, group_size), jnp.float32),
        jnp.zeros((tok_rows, kv_local, group_size, HD), jnp.float32),
    )
    key_piece = lax.all_gather(keys, "sp", axis=1, tiled=True)
    value_piece = lax.all_gather(values, "sp", axis=1, tiled=True)
    width_keys = key_piece.shape[1]
    key_cum = all_cache.reshape(kv_local, group_size, width_keys)

    def update(state):
        running_max, running_sum, numerator = state
        key_block = key_piece.reshape(kv_local, HD, width_keys)
        value_block = value_piece.reshape(kv_local, HD, width_keys)
        scores = (
            jnp.einsum("qagd,adk->qagk", grouped_q, key_block, preferred_element_type=jnp.float32)
            * score_scale
        )
        scores = scores + query_cum[..., None] - key_cum[None]
        key_pos = jnp.arange(width_keys, dtype=jnp.int32)
        allowed = (key_pos[None, :] <= query_pos[:, None]) & (
            doc_line[None, :] == documents[:, None]
        )
        allowed = allowed[:, None, None, :]
        scores = jnp.where(allowed, scores, masked_score)
        new_max = jnp.maximum(running_max, jnp.max(scores, axis=-1))
        weights = jnp.where(allowed, jnp.exp(scores - new_max[..., None]), 0.0)
        new_sum = jnp.sum(weights, axis=-1)
        added = jnp.einsum(
            "qagk,adk->qagd",
            weights.astype(jnp.bfloat16),
            value_block,
            preferred_element_type=jnp.float32,
        )
        return (new_max, new_sum, added)

    active = (jnp.int32(0) <= query_last) & (doc_line[width_keys - 1] >= documents[0])
    running_max, running_sum, numerator = lax.cond(active, update, lambda state: state, initial)
    attended = (
        (numerator / running_sum[..., None])
        .astype(jnp.bfloat16)
        .reshape(tok_rows, local_heads * HD)
    )
    token_heads = lax.all_to_all(attended, "tp", split_axis=0, concat_axis=1, tiled=True)
    mixed = jnp.dot(token_heads, out_weight, preferred_element_type=jnp.float32)
    mixed = lax.optimization_barrier(mixed.astype(jnp.bfloat16)).astype(jnp.float32)
    settled = normalize(residual_scale * residual.astype(jnp.float32) + mixed, mix_gain)
    row_count = settled.shape[0]
    width_model = settled.shape[1]
    top_count = routes.shape[1]
    expert_total = lax.axis_size(("sp", "tp")) * expert_gate.shape[0]
    capacity = row_count * lax.axis_size("tp") * top_count // expert_total
    chosen_experts = routes.reshape(-1)
    matches = (
        chosen_experts[:, None] == jnp.arange(expert_total, dtype=jnp.int32)[None, :]
    ).astype(jnp.int32)
    ranks = jnp.sum(jnp.cumsum(matches, axis=0) * matches, axis=1) - 1
    slots = chosen_experts * capacity + ranks
    placing = slots[None, :] == jnp.arange(expert_total * capacity, dtype=jnp.int32)[:, None]
    placing = jnp.any(
        placing.reshape(expert_total * capacity, row_count, top_count), axis=2
    ).astype(jnp.bfloat16)
    outgoing = jnp.dot(placing, settled, preferred_element_type=jnp.float32).astype(jnp.bfloat16)
    outgoing = outgoing.reshape(expert_total, capacity, width_model)
    finished = expert_block(
        lax.all_to_all(outgoing, ("sp", "tp"), split_axis=0, concat_axis=0, tiled=True),
        expert_gate,
        expert_up,
        expert_down,
    )
    returned = lax.all_to_all(finished, ("sp", "tp"), split_axis=0, concat_axis=0, tiled=True)
    returned = returned.reshape(expert_total * capacity, width_model)
    picked_rows = jnp.take(returned, slots, axis=0).reshape(row_count, top_count, width_model)
    routed = jnp.einsum("rkd,rk->rd", picked_rows.astype(jnp.float32), route_weight)
    shared_gate_part = jnp.dot(settled, shared_gate, preferred_element_type=jnp.float32)
    shared_up_part = jnp.dot(settled, shared_up, preferred_element_type=jnp.float32)
    shared_hidden = (jax.nn.silu(shared_gate_part) * shared_up_part).astype(jnp.bfloat16)
    shared = jnp.dot(shared_hidden, shared_down, preferred_element_type=jnp.float32)
    return normalize(residual_scale * settled.astype(jnp.float32) + routed + shared, ffn_gain)


def solution(mesh):
    placed = (
        P("sp", "tp"),
        P("tp", "sp"),
        P("tp", "sp"),
        P("tp", "sp"),
        P("sp"),
        P(("sp", "tp"), None),
        P(),
        P(),
        P(("sp", "tp"), None),
        P(("sp", "tp"), None),
        P(("sp", "tp"), None, None),
        P(("sp", "tp"), None, None),
        P(("sp", "tp"), None, None),
        P(),
        P(),
        P(),
        P(),
    )
    return jax.shard_map(
        local, mesh=mesh, in_specs=placed, out_specs=P(("sp", "tp"), None), check_vma=False
    )
```

profile of v0, /device:TPU:0, one launch (start us, length us, event | category | flops | bytes accessed | tf_op | source)
XLA Modules:
  0.0 393.6 jit_solution(2535516395564024456)
XLA Ops:
  6.5 0.0 copy-start
  6.5 0.0 all-gather.5.cloned.1.call-start
  6.5 1.7 copy.56
  8.3 0.0 all-gather.5.cloned.1.call-update
  8.3 0.0 all-gather.7.cloned.1.call-start
  8.3 0.7 all-gather.7.cloned.1.call-update
  9.0 0.8 copy.59
  9.8 0.1 eq.59
  9.9 0.1 reshape.234
  10.1 1.2 slice.14
  11.3 42.7 %all-gather.1 = s32[16,1,256]{2,1,0:T(1,128)S(1)} all-gather(s32[1,1,256]{2,1,0:T(1,128)} %bitcast.172), channel_id=2, replica_groups=mesh['sp'=16,'tp'=2] {'sp'}, dimensions={0}, use_global_device_ids=true | all-gather | bytes 17408 | tf_op jit(solution)/shard_map/all_gather | solution.py:64
  54.0 0.6 slice.19
  55.8 0.7 convert_element_type.60
  56.5 1.2 reduce-window.6
  57.7 0.2 slice_reduce_fusion
  58.0 0.1 fusion.50
  58.1 0.1 sub.47
  58.2 0.1 copy.62
  58.3 36.1 %all_gather.14 = f32[4,4096]{1,0:T(4,128)S(1)} all-gather(f32[4,256]{1,0:T(4,128)} %param.22), channel_id=1, replica_groups=mesh['sp'=16,'tp'=2] {'sp'}, dimensions={1}, use_global_device_ids=true | all-gather | bytes 69632 | tf_op jit(solution)/shard_map/all_gather | solution.py:63
  94.4 0.7 compare_and_fusion
  95.1 0.4 fusion.31
  95.4 0.0 all-gather.5.cloned.1.call-done
  95.4 29.3 %all-gather.7.cloned.1.call-done = bf16[128,4096]{1,0:T(8,128)(2,1)} async-done(((bf16[128,256]{1,0:T(8,128)(2,1)}), bf16[128,4096]{1,0:T(8,128)(2,1)}) %all-gather.7.cloned.1.call-update) | async-done | bytes 1048592 | tf_op jit(solution)/shard_map/all_gather | solution.py:73
  124.7 20.7 %conditional.1 = (f32[256,1,4]{0,2,1:T(4,128)S(1)}, f32[256,1,4,128]{3,0,2,1:T(8,128)S(1)}) conditional(s32[]{:T(128)} %convert_element_type.56, () %tuple.13, (s32[]{:T(128)}, s32[256]{0:T(256)S(1)}, s32[1,4096]{1,0:T(1,128)S(1)}, s32[256]{0:T(256)}, bf16[256,512]{1,0:T(8,128)(2,1)}, /*index=5*/bf16[128,4096]{0,1:T(8,128)(2,1)}, f32[256,4]{0,1:T(4,128)}, ...), branch_computations={%region_0.0_spmd, %region_1.4_spmd} | conditional | flops 2230320384 | bytes 61874252 | solution.py:104
  124.7 2.5 fusion.8
  127.3 0.0 copy-start.5
  127.3 0.0 copy-start.9
  127.3 5.5 %fusion.3 = (f32[256,4]{0,1:T(4,128)S(1)}, f32[4096,256,4]{1,0,2:T(8,128)S(1)}) fusion(f32[4,4096]{1,0:T(4,128)S(1)} %get-tuple-element.33, f32[256,4]{0,1:T(4,128)} %get-tuple-element.32, pred[256,4096]{0,1:T(8,128)(4,1)S(1)} %fusion.8, bf16[128,4096]{0,1:T(8,128)(2,1)} %get-tuple-element.30, bf16[256,512]{1,0:T(8,128)(2,1)} %get-tuple-element.40), kind=kOutput, calls=%fused_computation.7 | convolution fusion | flops 1094712320 | bytes 19210240 | tf_op jit(solution)/shard_map/cond/branch_1_fun/qagd,adk->qagk/dot_general | solution.py:82
  132.8 0.0 copy-done.5
  132.8 0.0 copy-done.9
  132.8 6.8 %fusion.9 = f32[256,1,4,128]{3,0,2,1:T(8,128)S(1)} fusion(f32[4096,256,4]{1,0,2:T(8,128)S(1)} %get-tuple-element.44, f32[256,4]{0,1:T(4,128)S(1)} %broadcast_maximum_fusion, f32[4,4096]{1,0:T(4,128)S(1)} %get-tuple-element.33, f32[256,4]{0,1:T(4,128)S(1)} %copy-done.5, pred[256,4096]{0,1:T(8,128)(4,1)S(1)} %fusion.8, bf16[128,4096]{1,0:T(8,128)(2,1)S(1)} %copy-done.9), kind=kOutput, calls=%fused_computation.13 | convolution fusion | flops 1103101952 | bytes 19472384 | tf_op jit(solution)/shard_map/cond/branch_1_fun/qagk,adk->qagd/dot_general | solution.py:95
  139.7 5.8 %fusion.2 = f32[256,4]{0,1:T(4,128)S(1)} fusion(f32[4096,256,4]{1,0,2:T(8,128)S(1)} %get-tuple-element.44, f32[256,4]{0,1:T(4,128)S(1)} %broadcast_maximum_fusion, f32[4,4096]{1,0:T(4,128)S(1)} %get-tuple-element.33, f32[256,4]{0,1:T(4,128)S(1)} %copy-done.5, pred[256,4096]{0,1:T(8,128)(4,1)S(1)} %fusion.8), kind=kLoop, calls=%fused_computation.6 | loop fusion | flops 29359104 | bytes 17903616 | tf_op jit(solution)/shard_map/cond/branch_1_fun/reduce_sum | solution.py:94
  145.5 0.0 copy-start.2
  145.5 0.2 divide_convert_fusion
  145.7 0.2 copy.57
  145.9 0.1 all_to_all.20
  146.0 3.9 %all_to_all.29 = bf16[2,128,512]{2,1,0:T(8,128)(2,1)S(1)} all-to-all(bf16[2,128,512]{2,1,0:T(8,128)(2,1)S(1)} %all_to_all.20), channel_id=1, replica_groups=mesh['sp'=16,'tp'=2] {'tp'}, dimensions={0} | all-to-all | bytes 524288 | tf_op jit(solution)/shard_map/all_to_all | solution.py:110
  149.9 0.2 copy.58
  150.1 2.9 convolution_convert_fusion.2
  153.1 0.0 copy-done.2
  153.1 0.3 fusion.40
  153.3 0.3 multiply_reduce_fusion.1
  153.7 0.3 multiply_convert_fusion.1
  154.0 0.0 copy-start.1
  154.0 1.2 convolution_convert_fusion.1
  155.2 0.0 copy-start.8
  155.2 96.7 %all_to_all.30 = bf16[32,32,2048]{2,1,0:T(8,128)(2,1)S(1)} all-to-all(bf16[32,32,2048]{2,1,0:T(8,128)(2,1)S(1)} %bitcast.161), channel_id=1, replica_groups=mesh['sp'=16,'tp'=2] {'sp','tp'}, dimensions={0} | all-to-all | bytes 8388608 | tf_op jit(solution)/shard_map/all_to_all | solution.py:132
  252.0 2.0 copy-done.3
  253.9 3.7 fusion.22
  257.7 0.0 copy-done
  257.7 10.1 %convolution_convert_fusion = bf16[32,32,2048]{2,1,0:T(8,128)(2,1)} fusion(bf16[1,512,2048]{2,1,0:T(8,128)(2,1)S(1)} %copy-done, f32[32,32,512]{2,1,0:T(8,128)} %fusion.22, bf16[32,32,2048]{2,1,0:T(8,128)(2,1)} %copy-done.3, bf16[1,2048,512]{2,1,0:T(8,128)(2,1)} %param.29), kind=kOutput, calls=%fused_computation.24 | convolution fusion | flops 4300210176 | bytes 14680064 | tf_op jit(solution)/shard_map/nemf,efd->nemd/dot_general | solution.py:29
  267.7 4.0 %all-to-all-start.2 = ((bf16[32,32,2048]{2,1,0:T(8,128)(2,1)}), bf16[32,32,2048]{2,1,0:T(8,128)(2,1)}, u32[]{:S(2)}, u32[]{:S(2)}) async-start(bf16[32,32,2048]{2,1,0:T(8,128)(2,1)} %convolution_convert_fusion), calls=%async_computation.2 | async-start | bytes 8388608 | tf_op jit(solution)/shard_map/all_to_all | solution.py:137
  271.8 0.1 copy.64
  271.9 0.1 mul.107
  272.0 0.1 copy.63
  272.2 0.2 copy.66
  272.4 2.0 fusion.58
  274.4 91.0 %all-to-all-done.2 = bf16[32,32,2048]{2,1,0:T(8,128)(2,1)} async-done(((bf16[32,32,2048]{2,1,0:T(8,128)(2,1)}), bf16[32,32,2048]{2,1,0:T(8,128)(2,1)}, u32[]{:S(2)}, u32[]{:S(2)}) %all-to-all-start.2) | async-done | bytes 4194336 | tf_op jit(solution)/shard_map/all_to_all | solution.py:137
  365.5 8.0 %gather_fusion = bf16[512,2048]{1,0:T(8,128)(2,1)} fusion(bf16[1024,2048]{1,0:T(8,128)(2,1)} %bitcast.35, s32[1024]{0:T(1024)S(1)} %pad_clamp_fusion), kind=kCustom, calls=%fused_computation | custom fusion | bytes 4196352 | tf_op jit(solution)/shard_map/jit(_take)/gather | solution.py:139
  373.5 4.1 %gather.7 = bf16[128,4,2048]{2,1,0:T(4,128)(2,1)} reshape(bf16[512,2048]{1,0:T(8,128)(2,1)} %gather_fusion) | data formatting | bytes 4194304 | tf_op jit(solution)/shard_map/jit(_take)/gather | solution.py:139
  377.6 3.9 fusion.29
  381.5 4.0 %fusion.57 = (f32[128]{0:T(128)S(1)}, f32[128,2048]{1,0:T(8,128)S(1)}) fusion(bf16[512,2048]{1,0:T(8,128)(2,1)} %param.34, bf16[128,2048]{1,0:T(8,128)(2,1)} %copy-done.1, bf16[2048,512]{1,0:T(8,128)(2,1)} %param.33, f32[128,512]{1,0:T(8,128)S(1)} %fusion.58, f32[128,1,2048]{2,1,0:T(1,128)} %fusion.29), kind=kOutput, calls=%fused_computation.85 | convolution fusion | flops 538574720 | bytes 7078400 | tf_op jit(solution)/shard_map/dot_general | solution.py:144
  385.5 0.3 multiply_reduce_fusion
  385.7 1.0 multiply_convert_fusion
  (24 shorter events, 0.1 us)
Async XLA Ops:
  6.5 251.1 %copy-start = (bf16[1,512,2048]{2,1,0:T(8,128)(2,1)S(1)}, bf16[1,512,2048]{2,1,0:T(8,128)(2,1)}, u32[]{:S(2)}) copy-start(bf16[1,512,2048]{2,1,0:T(8,128)(2,1)} %param.31) | copy-start | bytes 6291460
  6.5 88.9 %all-gather.5.cloned.1.call-start = ((), (), s32[]{:S(2)}) async-start(), calls=%async_computation.3 | async-start | bytes 1114112 | tf_op jit(solution)/shard_map/all_gather | solution.py:72
  8.3 116.4 %all-gather.7.cloned.1.call-start = ((), (), s32[]{:S(2)}) async-start(), calls=%async_computation.4 | async-start | bytes 1114112 | tf_op jit(solution)/shard_map/all_gather | solution.py:73
  127.3 5.5 %copy-start.5 = (f32[256,4]{0,1:T(4,128)S(1)}, f32[256,4]{0,1:T(4,128)}, u32[]{:S(2)}) copy-start(f32[256,4]{0,1:T(4,128)} %get-tuple-element.32) | copy-start | bytes 12292 | tf_op jit(solution)/shard_map/cond
  127.3 5.5 %copy-start.9 = (bf16[128,4096]{1,0:T(8,128)(2,1)S(1)}, bf16[128,4096]{1,0:T(8,128)(2,1)}, u32[]{:S(2)}) copy-start(bf16[128,4096]{1,0:T(8,128)(2,1)} %get-tuple-element.34) | copy-start | bytes 3145732 | tf_op jit(solution)/shard_map/cond
  145.5 7.6 %copy-start.2 = (bf16[128,2048]{1,0:T(8,128)(2,1)S(1)}, bf16[128,2048]{1,0:T(8,128)(2,1)}, u32[]{:S(2)}) copy-start(bf16[128,2048]{1,0:T(8,128)(2,1)} %param.24) | copy-start | bytes 1572868
  154.0 118.4 %copy-start.1 = (bf16[128,2048]{1,0:T(8,128)(2,1)}, bf16[128,2048]{1,0:T(8,128)(2,1)S(1)}, u32[]{:S(2)}) copy-start(bf16[128,2048]{1,0:T(8,128)(2,1)S(1)} %multiply_convert_fusion.1) | copy-start | bytes 1572868
  155.2 98.7 %copy-start.8 = (bf16[1,2048,512]{2,1,0:T(8,128)(2,1)S(1)}, bf16[1,2048,512]{2,1,0:T(8,128)(2,1)}, u32[]{:S(2)}) copy-start(bf16[1,2048,512]{2,1,0:T(8,128)(2,1)} %param.30) | copy-start | bytes 6291460
  252.0 2.0 copy-start.3
  267.7 4.0 %copy-start.4 = (s32[128,4]{0,1:T(4,128)S(1)}, s32[128,4]{0,1:T(4,128)}, u32[]{:S(2)}) copy-start(s32[128,4]{0,1:T(4,128)} %param.27) | copy-start | bytes 6148
  267.7 4.4 %copy-start.7 = (f32[128,4]{0,1:T(4,128)S(1)}, f32[128,4]{0,1:T(4,128)}, u32[]{:S(2)}) copy-start(f32[128,4]{0,1:T(4,128)} %param.28) | copy-start | bytes 6148
  267.7 4.6 %copy-start.6 = (bf16[2048]{0:T(1024)(128)(2,1)S(1)}, bf16[2048]{0:T(1024)(128)(2,1)}, u32[]{:S(2)}) copy-start(bf16[2048]{0:T(1024)(128)(2,1)} %param.35) | copy-start | bytes 12292
  267.7 97.7 %all-to-all-start.2 = ((bf16[32,32,2048]{2,1,0:T(8,128)(2,1)}), bf16[32,32,2048]{2,1,0:T(8,128)(2,1)}, u32[]{:S(2)}, u32[]{:S(2)}) async-start(bf16[32,32,2048]{2,1,0:T(8,128)(2,1)} %convolution_convert_fusion), calls=%async_computation.2 | async-start | bytes 8388608 | tf_op jit(solution)/shard_map/all_to_all | solution.py:137
Sparse Core Ops, SparseCore 0:
  10.1 57.9 all-gather.4
  70.8 53.9 all-gather.6
where the time goes:
time: 394 us
  blocking collectives  180 us (46%)
  waiting for transfers between devices  121 us (31%)
  matrix products  40.2 us (10%)
  local copies, waits for them, and re-layouts  20.1 us (5%)
  between operations  14.9 us (4%)
  other arithmetic  13.8 us (4%)
  starting transfers between devices  4.06 us (1%)
    all_to_all x1, blocking collectives, local(): lax.all_to_all(outgoing, ('sp', 'tp'), split_axis=0, concat_axis=0, tiled...  96.7 us
    all_to_all x1, waiting for transfers between devices, local(): lax.all_to_all(finished, ('sp', 'tp'), split_axis=0, concat_axis=0, tiled...  91 us
    all_gather x1, blocking collectives, local(): lax.all_gather(documents.reshape(1, tok_rows), 'sp', axis=1, tiled=True)  42.7 us
    all_gather x1, blocking collectives, local(): lax.all_gather(gate_cache, 'sp', axis=1, tiled=True)  36.1 us
    all_gather x1, waiting for transfers between devices, local(): value_piece = lax.all_gather(values, 'sp', axis=1, tiled=True)  29.3 us
    gather x2, local copies, waits for them, and re-layouts, local(): jnp.take(returned, slots, axis=0).reshape(row_count, top_count, width_model)  12.1 us
    dot_general x1, matrix products, expert_block(): jnp.einsum('nemf,efd->nemd', hidden, expert_down, preferred_element_type=...  10.1 us
  transfers between devices with their start and end apart: 3, of which 2 were waited for; matrix products, arithmetic and copies ran while one was open for 2% of the time, Pallas kernels for 0%

commit v1 on v0

--- a/solution.py
+++ b/solution.py
@@ -59,9 +59,13 @@
     query_last = seq_start + tok_rows - 1
     query_cum = jnp.transpose(gate_cache).reshape(tok_rows, kv_local, group_size)
     grouped_q = queries.reshape(tok_rows, kv_local, group_size, HD)
+
+    def keep_up_forms(slab_in, along_axis):
+        return jnp.concatenate(lax.all_gather(slab_in, along_axis), axis=1)
+
     all_cache, all_docs = (
         lax.all_gather(gate_cache, "sp", axis=1, tiled=True),
-        lax.all_gather(documents.reshape(1, tok_rows), "sp", axis=1, tiled=True),
+        keep_up_forms(documents.reshape(1, tok_rows), "sp"),
     )
     doc_line = all_docs[0]
     initial = (

time: 394 us -> 394 us (level)
  no operation moved by 1% of the time
where the time goes in v1:
time: 394 us
  blocking collectives  180 us (46%)
  waiting for transfers between devices  121 us (31%)
  matrix products  40.2 us (10%)
  local copies, waits for them, and re-layouts  20.1 us (5%)
  between operations  14.9 us (4%)
  other arithmetic  13.8 us (4%)
  starting transfers between devices  4.06 us (1%)
    all_to_all x1, blocking collectives, local(): lax.all_to_all(outgoing, ('sp', 'tp'), split_axis=0, concat_axis=0, tiled...  96.7 us
    all_to_all x1, waiting for transfers between devices, local(): lax.all_to_all(finished, ('sp', 'tp'), split_axis=0, concat_axis=0, tiled...  91 us
    all_gather x1, blocking collectives, keep_up_forms(): return jnp.concatenate(lax.all_gather(slab_in, along_axis), axis=1)  42.7 us
    all_gather x1, blocking collectives, local(): lax.all_gather(gate_cache, 'sp', axis=1, tiled=True)  36.1 us
    all_gather x1, waiting for transfers between devices, local(): value_piece = lax.all_gather(values, 'sp', axis=1, tiled=True)  29.3 us
    gather x2, local copies, waits for them, and re-layouts, local(): jnp.take(returned, slots, axis=0).reshape(row_count, top_count, width_model)  12.1 us
    dot_general x1, matrix products, expert_block(): jnp.einsum('nemf,efd->nemd', hidden, expert_down, preferred_element_type=...  10.1 us
  transfers between devices with their start and end apart: 3, of which 2 were waited for; matrix products, arithmetic and copies ran while one was open for 2% of the time, Pallas kernels for 0%

profile of v1, /device:TPU:0, one launch (start us, length us, event | category | flops | bytes accessed | tf_op | source)
XLA Modules:
  0.0 393.6 jit_solution(11862828123948388380)
XLA Ops:
  6.5 0.0 copy-start
  6.5 0.0 all-gather.5.cloned.1.call-start
  6.5 1.7 copy.56
  8.3 0.0 all-gather.5.cloned.1.call-update
  8.3 0.0 all-gather.7.cloned.1.call-start
  8.3 0.7 all-gather.7.cloned.1.call-update
  9.0 0.8 copy.59
  9.8 0.1 eq.59
  9.9 0.1 reshape.231
  10.1 1.2 slice.13
  11.3 42.7 %all-gather.1 = s32[16,1,256]{2,1,0:T(1,128)S(1)} all-gather(s32[1,1,256]{2,1,0:T(1,128)} %bitcast.170), channel_id=2, replica_groups=mesh['sp'=16,'tp'=2] {'sp'}, dimensions={0}, use_global_device_ids=true | all-gather | bytes 17408 | tf_op jit(solution)/shard_map/all_gather | solution.py:64
  54.0 0.6 slice.19
  55.8 0.7 convert_element_type.60
  56.5 1.2 reduce-window.6
  57.7 0.2 slice_reduce_fusion
  58.0 0.1 fusion.50
  58.1 0.1 sub.47
  58.2 0.1 copy.62
  58.3 36.1 %all_gather.14 = f32[4,4096]{1,0:T(4,128)S(1)} all-gather(f32[4,256]{1,0:T(4,128)} %param.22), channel_id=1, replica_groups=mesh['sp'=16,'tp'=2] {'sp'}, dimensions={1}, use_global_device_ids=true | all-gather | bytes 69632 | tf_op jit(solution)/shard_map/all_gather | solution.py:67
  94.4 0.7 compare_and_fusion
  95.1 0.4 fusion.31
  95.4 0.0 all-gather.5.cloned.1.call-done
  95.4 29.3 %all-gather.7.cloned.1.call-done = bf16[128,4096]{1,0:T(8,128)(2,1)} async-done(((bf16[128,256]{1,0:T(8,128)(2,1)}), bf16[128,4096]{1,0:T(8,128)(2,1)}) %all-gather.7.cloned.1.call-update) | async-done | bytes 1048592 | tf_op jit(solution)/shard_map/all_gather | solution.py:77
  124.7 20.7 %conditional.1 = (f32[256,1,4]{0,2,1:T(4,128)S(1)}, f32[256,1,4,128]{3,0,2,1:T(8,128)S(1)}) conditional(s32[]{:T(128)} %convert_element_type.56, () %tuple.13, (s32[]{:T(128)}, s32[256]{0:T(256)S(1)}, s32[16,1,256]{2,1,0:T(1,128)S(1)}, s32[256]{0:T(256)}, bf16[256,512]{1,0:T(8,128)(2,1)}, /*index=5*/bf16[128,4096]{0,1:T(8,128)(2,1)}, ...), branch_computations={%region_0.0_spmd, %region_1.4_spmd} | conditional | flops 2230320384 | bytes 61874252 | solution.py:108
  124.7 2.5 fusion.8
  127.3 0.0 copy-start.5
  127.3 0.0 copy-start.9
  127.3 5.5 %fusion.3 = (f32[256,4]{0,1:T(4,128)S(1)}, f32[4096,256,4]{1,0,2:T(8,128)S(1)}) fusion(f32[4,4096]{1,0:T(4,128)S(1)} %get-tuple-element.33, f32[256,4]{0,1:T(4,128)} %get-tuple-element.32, pred[256,4096]{0,1:T(8,128)(4,1)S(1)} %fusion.8, bf16[128,4096]{0,1:T(8,128)(2,1)} %get-tuple-element.30, bf16[256,512]{1,0:T(8,128)(2,1)} %get-tuple-element.40), kind=kOutput, calls=%fused_computation.7 | convolution fusion | flops 1094712320 | bytes 19210240 | tf_op jit(solution)/shard_map/cond/branch_1_fun/qagd,adk->qagk/dot_general | solution.py:86
  132.8 0.0 copy-done.5
  132.8 0.0 copy-done.9
  132.8 6.8 %fusion.9 = f32[256,1,4,128]{3,0,2,1:T(8,128)S(1)} fusion(f32[4096,256,4]{1,0,2:T(8,128)S(1)} %get-tuple-element.44, f32[256,4]{0,1:T(4,128)S(1)} %broadcast_maximum_fusion, f32[4,4096]{1,0:T(4,128)S(1)} %get-tuple-element.33, f32[256,4]{0,1:T(4,128)S(1)} %copy-done.5, pred[256,4096]{0,1:T(8,128)(4,1)S(1)} %fusion.8, bf16[128,4096]{1,0:T(8,128)(2,1)S(1)} %copy-done.9), kind=kOutput, calls=%fused_computation.13 | convolution fusion | flops 1103101952 | bytes 19472384 | tf_op jit(solution)/shard_map/cond/branch_1_fun/qagk,adk->qagd/dot_general | solution.py:99
  139.7 5.8 %fusion.2 = f32[256,4]{0,1:T(4,128)S(1)} fusion(f32[4096,256,4]{1,0,2:T(8,128)S(1)} %get-tuple-element.44, f32[256,4]{0,1:T(4,128)S(1)} %broadcast_maximum_fusion, f32[4,4096]{1,0:T(4,128)S(1)} %get-tuple-element.33, f32[256,4]{0,1:T(4,128)S(1)} %copy-done.5, pred[256,4096]{0,1:T(8,128)(4,1)S(1)} %fusion.8), kind=kLoop, calls=%fused_computation.6 | loop fusion | flops 29359104 | bytes 17903616 | tf_op jit(solution)/shard_map/cond/branch_1_fun/reduce_sum | solution.py:98
  145.5 0.0 copy-start.2
  145.5 0.2 divide_convert_fusion
  145.7 0.2 copy.57
  145.9 0.1 all_to_all.20
  146.0 3.9 %all_to_all.29 = bf16[2,128,512]{2,1,0:T(8,128)(2,1)S(1)} all-to-all(bf16[2,128,512]{2,1,0:T(8,128)(2,1)S(1)} %all_to_all.20), channel_id=1, replica_groups=mesh['sp'=16,'tp'=2] {'tp'}, dimensions={0} | all-to-all | bytes 524288 | tf_op jit(solution)/shard_map/all_to_all | solution.py:114
  149.9 0.2 copy.58
  150.1 2.9 convolution_convert_fusion.2
  153.1 0.0 copy-done.2
  153.1 0.3 fusion.40
  153.3 0.3 multiply_reduce_fusion.1
  153.7 0.3 multiply_convert_fusion.1
  154.0 0.0 copy-start.1
  154.0 1.2 convolution_convert_fusion.1
  155.2 0.0 copy-start.8
  155.2 96.7 %all_to_all.30 = bf16[32,32,2048]{2,1,0:T(8,128)(2,1)S(1)} all-to-all(bf16[32,32,2048]{2,1,0:T(8,128)(2,1)S(1)} %bitcast.160), channel_id=1, replica_groups=mesh['sp'=16,'tp'=2] {'sp','tp'}, dimensions={0} | all-to-all | bytes 8388608 | tf_op jit(solution)/shard_map/all_to_all | solution.py:136
  252.0 2.0 copy-done.3
  253.9 3.7 fusion.22
  257.7 0.0 copy-done
  257.7 10.1 %convolution_convert_fusion = bf16[32,32,2048]{2,1,0:T(8,128)(2,1)} fusion(bf16[1,512,2048]{2,1,0:T(8,128)(2,1)S(1)} %copy-done, f32[32,32,512]{2,1,0:T(8,128)} %fusion.22, bf16[32,32,2048]{2,1,0:T(8,128)(2,1)} %copy-done.3, bf16[1,2048,512]{2,1,0:T(8,128)(2,1)} %param.29), kind=kOutput, calls=%fused_computation.24 | convolution fusion | flops 4300210176 | bytes 14680064 | tf_op jit(solution)/shard_map/nemf,efd->nemd/dot_general | solution.py:29
  267.7 4.0 %all-to-all-start.2 = ((bf16[32,32,2048]{2,1,0:T(8,128)(2,1)}), bf16[32,32,2048]{2,1,0:T(8,128)(2,1)}, u32[]{:S(2)}, u32[]{:S(2)}) async-start(bf16[32,32,2048]{2,1,0:T(8,128)(2,1)} %convolution_convert_fusion), calls=%async_computation.2 | async-start | bytes 8388608 | tf_op jit(solution)/shard_map/all_to_all | solution.py:141
  271.8 0.1 copy.64
  271.9 0.1 mul.107
  272.0 0.1 copy.63
  272.2 0.2 copy.66
  272.4 2.0 fusion.58
  274.4 91.0 %all-to-all-done.2 = bf16[32,32,2048]{2,1,0:T(8,128)(2,1)} async-done(((bf16[32,32,2048]{2,1,0:T(8,128)(2,1)}), bf16[32,32,2048]{2,1,0:T(8,128)(2,1)}, u32[]{:S(2)}, u32[]{:S(2)}) %all-to-all-start.2) | async-done | bytes 4194336 | tf_op jit(solution)/shard_map/all_to_all | solution.py:141
  365.5 8.0 %gather_fusion = bf16[512,2048]{1,0:T(8,128)(2,1)} fusion(bf16[1024,2048]{1,0:T(8,128)(2,1)} %bitcast.34, s32[1024]{0:T(1024)S(1)} %pad_clamp_fusion), kind=kCustom, calls=%fused_computation | custom fusion | bytes 4196352 | tf_op jit(solution)/shard_map/jit(_take)/gather | solution.py:143
  373.5 4.1 %gather.7 = bf16[128,4,2048]{2,1,0:T(4,128)(2,1)} reshape(bf16[512,2048]{1,0:T(8,128)(2,1)} %gather_fusion) | data formatting | bytes 4194304 | tf_op jit(solution)/shard_map/jit(_take)/gather | solution.py:143
  377.6 3.9 fusion.29
  381.5 4.0 %fusion.57 = (f32[128]{0:T(128)S(1)}, f32[128,2048]{1,0:T(8,128)S(1)}) fusion(bf16[512,2048]{1,0:T(8,128)(2,1)} %param.34, bf16[128,2048]{1,0:T(8,128)(2,1)} %copy-done.1, bf16[2048,512]{1,0:T(8,128)(2,1)} %param.33, f32[128,512]{1,0:T(8,128)S(1)} %fusion.58, f32[128,1,2048]{2,1,0:T(1,128)} %fusion.29), kind=kOutput, calls=%fused_computation.85 | convolution fusion | flops 538574720 | bytes 7078400 | tf_op jit(solution)/shard_map/dot_general | solution.py:148
  385.5 0.3 multiply_reduce_fusion
  385.7 1.0 multiply_convert_fusion
  (24 shorter events, 0.1 us)
Async XLA Ops:
  6.5 251.1 %copy-start = (bf16[1,512,2048]{2,1,0:T(8,128)(2,1)S(1)}, bf16[1,512,2048]{2,1,0:T(8,128)(2,1)}, u32[]{:S(2)}) copy-start(bf16[1,512,2048]{2,1,0:T(8,128)(2,1)} %param.31) | copy-start | bytes 6291460
  6.5 88.9 %all-gather.5.cloned.1.call-start = ((), (), s32[]{:S(2)}) async-start(), calls=%async_computation.3 | async-start | bytes 1114112 | tf_op jit(solution)/shard_map/all_gather | solution.py:76
  8.3 116.4 %all-gather.7.cloned.1.call-start = ((), (), s32[]{:S(2)}) async-start(), calls=%async_computation.4 | async-start | bytes 1114112 | tf_op jit(solution)/shard_map/all_gather | solution.py:77
  127.3 5.5 %copy-start.5 = (f32[256,4]{0,1:T(4,128)S(1)}, f32[256,4]{0,1:T(4,128)}, u32[]{:S(2)}) copy-start(f32[256,4]{0,1:T(4,128)} %get-tuple-element.32) | copy-start | bytes 12292 | tf_op jit(solution)/shard_map/cond
  127.3 5.5 %copy-start.9 = (bf16[128,4096]{1,0:T(8,128)(2,1)S(1)}, bf16[128,4096]{1,0:T(8,128)(2,1)}, u32[]{:S(2)}) copy-start(bf16[128,4096]{1,0:T(8,128)(2,1)} %get-tuple-element.34) | copy-start | bytes 3145732 | tf_op jit(solution)/shard_map/cond
  145.5 7.6 %copy-start.2 = (bf16[128,2048]{1,0:T(8,128)(2,1)S(1)}, bf16[128,2048]{1,0:T(8,128)(2,1)}, u32[]{:S(2)}) copy-start(bf16[128,2048]{1,0:T(8,128)(2,1)} %param.24) | copy-start | bytes 1572868
  154.0 118.4 %copy-start.1 = (bf16[128,2048]{1,0:T(8,128)(2,1)}, bf16[128,2048]{1,0:T(8,128)(2,1)S(1)}, u32[]{:S(2)}) copy-start(bf16[128,2048]{1,0:T(8,128)(2,1)S(1)} %multiply_convert_fusion.1) | copy-start | bytes 1572868
  155.2 98.7 %copy-start.8 = (bf16[1,2048,512]{2,1,0:T(8,128)(2,1)S(1)}, bf16[1,2048,512]{2,1,0:T(8,128)(2,1)}, u32[]{:S(2)}) copy-start(bf16[1,2048,512]{2,1,0:T(8,128)(2,1)} %param.30) | copy-start | bytes 6291460
  252.0 2.0 copy-start.3
  267.7 4.0 %copy-start.4 = (s32[128,4]{0,1:T(4,128)S(1)}, s32[128,4]{0,1:T(4,128)}, u32[]{:S(2)}) copy-start(s32[128,4]{0,1:T(4,128)} %param.27) | copy-start | bytes 6148
  267.7 4.4 %copy-start.7 = (f32[128,4]{0,1:T(4,128)S(1)}, f32[128,4]{0,1:T(4,128)}, u32[]{:S(2)}) copy-start(f32[128,4]{0,1:T(4,128)} %param.28) | copy-start | bytes 6148
  267.7 4.6 %copy-start.6 = (bf16[2048]{0:T(1024)(128)(2,1)S(1)}, bf16[2048]{0:T(1024)(128)(2,1)}, u32[]{:S(2)}) copy-start(bf16[2048]{0:T(1024)(128)(2,1)} %param.35) | copy-start | bytes 12292
  267.7 97.7 %all-to-all-start.2 = ((bf16[32,32,2048]{2,1,0:T(8,128)(2,1)}), bf16[32,32,2048]{2,1,0:T(8,128)(2,1)}, u32[]{:S(2)}, u32[]{:S(2)}) async-start(bf16[32,32,2048]{2,1,0:T(8,128)(2,1)} %convolution_convert_fusion), calls=%async_computation.2 | async-start | bytes 8388608 | tf_op jit(solution)/shard_map/all_to_all | solution.py:141
Sparse Core Ops, SparseCore 0:
  10.1 57.9 all-gather.4
  70.8 53.9 all-gather.6
